TPU v7x, 32 devices: a whole 2x2x4 slice. The times are simulated.
32 devices in a mesh: ep: 8 (over z, x), tp: 4 (over y, core).
Axes of the slice: x: 2, y: 2, z: 4, core: 2. Of those that a mesh axis runs over, the one named last changes fastest.
Arguments:
- tokens: bfloat16 [512, 4096], P('ep'), may hold values from -6 to 6
- state_in: float32 [512, 4096], P('ep', 'tp'), may hold values from -6 to 6
- conv_in: bfloat16 [512, 3, 4096], P('ep', None, 'tp'), may hold values from -6 to 6
- mix_gain: bfloat16 [4096], replicated, may hold values from 0.099609375 to 1.8984375
- rnn_weight: bfloat16 [4096, 4096], P('ep', 'tp'), may hold values from -0.09375 to 0.09375
- gate_weight: bfloat16 [4096, 4096], P('ep', 'tp'), may hold values from -0.09375 to 0.09375
- conv_weight: bfloat16 [4, 4096], P(None, 'tp'), may hold values from -3 to 3
- rate_weight: bfloat16 [16, 256, 256], P('tp'), may hold values from -0.375 to 0.375
- input_weight: bfloat16 [16, 256, 256], P('tp'), may hold values from -0.375 to 0.375
- rate_param: float32 [4096], P('tp'), may hold values from 1 to 6
- out_weight: bfloat16 [4096, 4096], P('tp'), may hold values from -0.09375 to 0.09375
- moe_gain: bfloat16 [4096], replicated, may hold values from 0.099609375 to 1.8984375
- expert_gate: bfloat16 [8, 4096, 2048], P('ep', None, 'tp'), may hold values from -0.09375 to 0.09375
- expert_up: bfloat16 [8, 4096, 2048], P('ep', None, 'tp'), may hold values from -0.09375 to 0.09375
- expert_down: bfloat16 [8, 2048, 4096], P('ep', 'tp'), may hold values from -0.125 to 0.125
- routes: int32 [512, 2], P('ep'), may hold values from 0 to 7, all different within a row; in each aligned block of 64 rows (0 to 63, 64 to 127, ...) at most 32 rows name the same one
- route_prob: float32 [512, 2], P('ep'), may hold values from 0.1 to 1
Outputs:
- layer_out: bfloat16 [512, 4096], P('ep', 'tp')
- state_out: float32 [512, 4096], P('ep', 'tp')
- conv_out: bfloat16 [512, 3, 4096], P('ep', None, 'tp')
Inputs may be any that keep to these rules, and one draw needn't show every extreme that they name: `routes`: the 2 experts of a sequence differ. Among the rows of one index of ep no expert is named more than 32 times, and in every draw some expert is named exactly 32 times there.
All inputs are finite; a program needn't handle non-finite values.
Results may differ from a plain program's by a relative error of at most 0.014.
Values may be sent and summed in bfloat16 or wider, within the bound.
A program may use at most 64 MiB of HBM per device.

v0:
```python
import jax
import jax.numpy as jnp
from jax import lax
from jax.sharding import PartitionSpec as P


def rms_scale(values, gain):
    scale = lax.rsqrt(jnp.mean(values * values, axis=-1, keepdims=True) + 1e-06)
    return values * scale * gain.astype(jnp.float32)


def slot_targets(route_ids, experts, capacity):
    flat_ids = route_ids.reshape(-1)
    onehot = (flat_ids[:, None] == jnp.arange(experts, dtype=jnp.int32)[None, :]).astype(jnp.int32)
    before = jnp.cumsum(onehot, axis=0) - onehot
    slot_ids = jnp.sum(before * onehot, axis=1)
    return flat_ids * capacity + slot_ids


def block_map(conv, weight):
    rows = conv.shape[0]
    blocks = weight.shape[0]
    parts = conv.reshape(rows, blocks, weight.shape[1])
    mapped = jnp.einsum("snc,ncd->snd", parts, weight, preferred_element_type=jnp.float32)
    return mapped.reshape(rows, blocks * weight.shape[2])


def shards(
    tokens,
    state_in,
    conv_in,
    mix_gain,
    rnn_weight,
    gate_weight,
    conv_weight,
    rate_weight,
    input_weight,
    rate_param,
    out_weight,
    moe_gain,
    expert_gate,
    expert_up,
    expert_down,
    routes,
    route_prob,
):
    group_rows = tokens.shape[0]
    model_width = tokens.shape[1]
    channels = rnn_weight.shape[1]
    base = tokens.astype(jnp.float32)
    normed = rms_scale(base, mix_gain).astype(jnp.bfloat16)
    columns = lax.all_to_all(normed, "ep", split_axis=1, concat_axis=0, tiled=True)
    joined = jnp.concatenate([rnn_weight, gate_weight], axis=1)
    summed = lax.psum_scatter(
        jnp.dot(columns, joined, preferred_element_type=jnp.float32).astype(jnp.bfloat16),
        "ep",
        scatter_dimension=0,
        tiled=True,
    ).astype(jnp.float32)
    proj_x = summed[:, :channels]
    proj_y = summed[:, channels:]
    moved = proj_x.astype(jnp.bfloat16)
    conv_out = jnp.concatenate([conv_in[:, 1:], moved[:, None, :]], axis=1)
    taps = conv_weight.astype(jnp.float32)
    history = conv_in.astype(jnp.float32)
    mixed_in = (
        history[:, 0] * taps[0]
        + history[:, 1] * taps[1]
        + history[:, 2] * taps[2]
        + moved.astype(jnp.float32) * taps[3]
    )
    conv = mixed_in.astype(jnp.bfloat16)
    rate = jax.nn.sigmoid(block_map(conv, rate_weight))
    in_gate = jax.nn.sigmoid(block_map(conv, input_weight))
    log_decay = -8.0 * rate * jax.nn.softplus(-rate_param)
    state_out = jnp.exp(log_decay) * state_in + jnp.sqrt(
        -jnp.expm1(2.0 * log_decay)
    ) * in_gate * conv.astype(jnp.float32)
    gated = (state_out * jax.nn.gelu(proj_y, approximate=True)).astype(jnp.bfloat16)
    partial_out = jnp.dot(gated, out_weight, preferred_element_type=jnp.float32)
    mixed = base + lax.psum(partial_out.astype(jnp.bfloat16), "tp").astype(jnp.float32)
    normed2 = rms_scale(mixed, moe_gain).astype(jnp.bfloat16)
    experts = lax.axis_size("ep")
    topk = routes.shape[1]
    capacity = max(2, 2 * group_rows * topk // experts)
    targets = slot_targets(routes, experts, capacity)
    dispatch = (
        jnp.arange(experts * capacity, dtype=jnp.int32)[:, None] == targets[None, :]
    ).astype(jnp.bfloat16)
    repeated = jnp.repeat(normed2, topk, axis=0)
    send = jnp.dot(dispatch, repeated, preferred_element_type=jnp.float32).astype(jnp.bfloat16)
    send = send.reshape(experts, capacity, model_width)
    received = lax.all_to_all(send, "ep", split_axis=0, concat_axis=0, tiled=True)
    flat_rows = received.reshape(-1, model_width)
    gate_part = jnp.dot(flat_rows, expert_gate[0], preferred_element_type=jnp.float32)
    up_part = jnp.dot(flat_rows, expert_up[0], preferred_element_type=jnp.float32)
    hidden = (jax.nn.silu(gate_part) * up_part).astype(jnp.bfloat16)
    result = jnp.dot(hidden, expert_down[0], preferred_element_type=jnp.float32)
    partial_experts = result.reshape(received.shape[0], received.shape[1], model_width)
    reduced = lax.psum_scatter(
        partial_experts.astype(jnp.bfloat16), "tp", scatter_dimension=2, tiled=True
    )
    returned = lax.all_to_all(reduced, "ep", split_axis=0, concat_axis=0, tiled=True)
    share = returned.shape[2]
    picked = jnp.einsum(
        "rj,rd->jd",
        dispatch,
        returned.reshape(experts * capacity, share),
        preferred_element_type=jnp.float32,
    )
    weights = route_prob / jnp.sum(route_prob, axis=1, keepdims=True)
    experts_sum = jnp.sum(picked.reshape(group_rows, topk, share) * weights[:, :, None], axis=1)
    own_columns = lax.dynamic_slice_in_dim(mixed, lax.axis_index("tp") * share, share, 1)
    layer_out = (own_columns + experts_sum).astype(jnp.bfloat16)
    return (layer_out, state_out, conv_out)


def solution(mesh):
    in_specs = (
        P("ep", None),
        P("ep", "tp"),
        P("ep", None, "tp"),
        P(),
        P("ep", "tp"),
        P("ep", "tp"),
        P(None, "tp"),
        P("tp", None, None),
        P("tp", None, None),
        P("tp"),
        P("tp", None),
        P(),
        P("ep", None, "tp"),
        P("ep", None, "tp"),
        P("ep", "tp", None),
        P("ep", None),
        P("ep", None),
    )
    out_specs = (P("ep", "tp"), P("ep", "tp"), P("ep", None, "tp"))
    return jax.shard_map(shards, mesh=mesh, in_specs=in_specs, out_specs=out_specs, check_vma=False)
```

profile of v0, /device:TPU:0, one launch (start us, length us, event | category | flops | bytes accessed | tf_op | source)
XLA Modules:
  0.0 267.9 jit_solution(9502218566155616131)
XLA Ops:
  7.2 0.0 copy-start
  7.2 0.0 reduce-scatter.3.cloned.1.call-start
  7.2 0.7 convert_element_type.63
  8.0 1.2 fusion.23
  9.2 1.2 fusion.25
  10.5 21.6 %all_to_all.29 = bf16[64,8,512]{2,0,1:T(8,128)(2,1)S(1)} all-to-all(bf16[64,8,512]{2,0,1:T(8,128)(2,1)S(1)} %bitcast.85), channel_id=1, replica_groups=mesh['ep'=8,'tp'=4] {'ep'}, dimensions={1} | all-to-all | bytes 1048576 | tf_op jit(solution)/shard_map/all_to_all | solution.py:52
  32.1 4.2 %convolution_convert_fusion.3 = bf16[512,2048]{1,0:T(8,128)(2,1)} fusion(bf16[512,512]{1,0:T(8,128)(2,1)S(1)} %bitcast.88, bf16[512,1024]{1,0:T(8,128)(2,1)} %param.22, bf16[512,1024]{1,0:T(8,128)(2,1)} %param.21), kind=kOutput, calls=%fused_computation.8 | convolution fusion | flops 1078984704 | bytes 4718592 | tf_op jit(solution)/shard_map/dot_general | solution.py:55
  36.3 0.0 reduce-scatter.3.cloned.1.call-update
  36.4 0.0 all-reduce.2.cloned.1.call-start
  36.4 0.0 copy-done.3
  36.4 0.1 convert_element_type.61
  36.5 0.1 copy.30
  36.6 0.1 reshape.101
  36.7 0.1 fusion.52
  36.8 0.2 reduce_window_sum.11
  37.1 66.8 %reduce-scatter.3.cloned.1.call-done = bf16[64,2048]{1,0:T(8,128)(2,1)} async-done(((bf16[512,2048]{1,0:T(8,128)(2,1)}), bf16[64,2048]{1,0:T(8,128)(2,1)}) %reduce-scatter.3.cloned.1.call-update) | async-done | bytes 262160 | tf_op jit(solution)/shard_map/reduce_scatter | solution.py:54
  103.8 1.1 fusion.36
  104.9 0.2 fusion.22
  105.2 0.2 fusion.18
  105.5 0.2 multiply_add_fusion
  105.7 0.0 copy-start.2
  105.7 0.0 copy-start.7
  105.8 0.0 copy-start.1
  105.8 5.9 %convolution_convert_fusion.2 = bf16[64,4096]{1,0:T(8,128)(2,1)} fusion(bf16[1024,4096]{1,0:T(8,128)(2,1)} %param.27, f32[64,1024]{1,0:T(8,128)S(1)} %multiply_add_fusion, bf16[64,2048]{1,0:T(8,128)(2,1)S(1)} %copy-done.4), kind=kOutput, calls=%fused_computation.2 | convolution fusion | flops 537853952 | bytes 9306112 | tf_op jit(solution)/shard_map/dot_general | solution.py:80
  111.7 0.0 all-reduce.2.cloned.1.call-update
  111.7 0.0 reduce-scatter.5.cloned.1.call-start
  111.7 0.2 select_reduce_fusion
  111.9 32.4 %all-reduce.2.cloned.1.call-done = bf16[64,4096]{1,0:T(8,128)(2,1)} async-done(((bf16[64,4096]{1,0:T(8,128)(2,1)}), bf16[64,4096]{1,0:T(8,128)(2,1)}) %all-reduce.2.cloned.1.call-update) | async-done | bytes 524304 | tf_op jit(solution)/shard_map/psum | solution.py:81
  144.3 2.3 convert_add_fusion
  146.6 1.3 multiply_convert_fusion
  147.9 1.0 broadcast_in_dim.4
  148.9 0.4 reshape.102
  149.3 0.0 copy-start.11
  149.4 0.7 convolution_convert_fusion
  150.1 52.8 %all_to_all.30 = bf16[8,32,4096]{2,1,0:T(8,128)(2,1)S(1)} all-to-all(bf16[8,32,4096]{2,1,0:T(8,128)(2,1)S(1)} %bitcast.80), channel_id=1, replica_groups=mesh['ep'=8,'tp'=4] {'ep'}, dimensions={0} | all-to-all | bytes 4194304 | tf_op jit(solution)/shard_map/all_to_all | solution.py:93
  202.9 1.2 fusion.3
  204.1 0.9 copy-done.12
  205.1 1.3 fusion.11
  206.3 0.9 copy-done.13
  207.2 2.6 convolution_convert_fusion.1
  209.8 0.0 reduce-scatter.5.cloned.1.call-update
  209.9 29.8 %reduce-scatter.5.cloned.1.call-done = bf16[8,32,1024]{2,1,0:T(8,128)(2,1)} async-done(((bf16[8,32,4096]{2,1,0:T(8,128)(2,1)}), bf16[8,32,1024]{2,1,0:T(8,128)(2,1)}) %reduce-scatter.5.cloned.1.call-update) | async-done | bytes 524304 | tf_op jit(solution)/shard_map/reduce_scatter | solution.py:100
  239.7 5.5 %all-to-all-start.2 = ((bf16[8,32,1024]{2,1,0:T(8,128)(2,1)}), bf16[8,32,1024]{2,1,0:T(8,128)(2,1)S(1)}, u32[]{:S(2)}, u32[]{:S(2)}) async-start(bf16[8,32,1024]{2,1,0:T(8,128)(2,1)} %reduce-scatter.5.cloned.1.call-done), calls=%async_computation.4 | async-start | bytes 1048576 | tf_op jit(solution)/shard_map/all_to_all | solution.py:103
  245.2 0.1 iota_compare_fusion.1
  245.4 0.8 pad_maximum_fusion
  246.2 13.3 %all-to-all-done.2 = bf16[8,32,1024]{2,1,0:T(8,128)(2,1)S(1)} async-done(((bf16[8,32,1024]{2,1,0:T(8,128)(2,1)}), bf16[8,32,1024]{2,1,0:T(8,128)(2,1)S(1)}, u32[]{:S(2)}, u32[]{:S(2)}) %all-to-all-start.2) | async-done | bytes 524320 | tf_op jit(solution)/shard_map/all_to_all | solution.py:103
  259.5 0.2 fusion.14
  259.7 1.6 add_convert_fusion
  (37 shorter events, 0.2 us)
Async XLA Ops:
  7.2 97.7 %copy-start = (bf16[4,256,256]{2,1,0:T(8,128)(2,1)S(1)}, bf16[4,256,256]{2,1,0:T(8,128)(2,1)}, u32[]{:S(2)}) copy-start(bf16[4,256,256]{2,1,0:T(8,128)(2,1)} %param.24) | copy-start | bytes 1572868
  7.2 96.7 %reduce-scatter.3.cloned.1.call-start = ((), (), s32[]{:S(2)}) async-start(), calls=%async_computation.5 | async-start | bytes 2359296 | tf_op jit(solution)/shard_map/reduce_scatter | solution.py:54
  32.1 4.3 %copy-start.3 = (bf16[64,3,1024]{2,0,1:T(8,128)(2,1)S(1)}, bf16[64,3,1024]{2,0,1:T(8,128)(2,1)}, u32[]{:S(2)}) copy-start(bf16[64,3,1024]{2,0,1:T(8,128)(2,1)} %param.19) | copy-start | bytes 1179652
  32.1 4.4 %copy-start.10 = (s32[64,2]{0,1:T(2,128)S(1)}, s32[64,2]{0,1:T(2,128)}, u32[]{:S(2)}) copy-start(s32[64,2]{0,1:T(2,128)} %param.32) | copy-start | bytes 1540
  32.1 4.9 %copy-start.8 = (f32[1024]{0:T(1024)S(1)}, f32[1024]{0:T(1024)}, u32[]{:S(2)}) copy-start(f32[1024]{0:T(1024)} %param.26) | copy-start | bytes 12292
  32.1 4.9 %copy-start.6 = (bf16[4,1024]{1,0:T(4,128)(2,1)S(1)}, bf16[4,1024]{1,0:T(4,128)(2,1)}, u32[]{:S(2)}) copy-start(bf16[4,1024]{1,0:T(4,128)(2,1)} %param.23) | copy-start | bytes 24580
  36.3 68.9 %copy-start.14 = (bf16[4,256,256]{2,1,0:T(8,128)(2,1)S(1)}, bf16[4,256,256]{2,1,0:T(8,128)(2,1)}, u32[]{:S(2)}) copy-start(bf16[4,256,256]{2,1,0:T(8,128)(2,1)} %param.25) | copy-start | bytes 1572868
  36.3 69.2 %copy-start.5 = (f32[64,1024]{1,0:T(8,128)S(1)}, f32[64,1024]{1,0:T(8,128)}, u32[]{:S(2)}) copy-start(f32[64,1024]{1,0:T(8,128)} %param.18) | copy-start | bytes 786436
  36.4 107.9 %all-reduce.2.cloned.1.call-start = ((), (), s32[]{:S(2)}) async-start(), calls=%async_computation.6 | async-start | bytes 1048576 | tf_op jit(solution)/shard_map/psum | solution.py:81
  103.8 1.9 copy-start.4
  105.7 5.9 %copy-start.2 = (f32[64,1024]{1,0:T(8,128)}, f32[64,1024]{1,0:T(8,128)S(1)}, u32[]{:S(2)}) copy-start(f32[64,1024]{1,0:T(8,128)S(1)} %multiply_add_fusion) | copy-start | bytes 786436
  105.7 6.2 %copy-start.7 = (bf16[4096]{0:T(1024)(128)(2,1)S(1)}, bf16[4096]{0:T(1024)(128)(2,1)}, u32[]{:S(2)}) copy-start(bf16[4096]{0:T(1024)(128)(2,1)} %param.28) | copy-start | bytes 24580
  105.8 38.5 %copy-start.1 = (bf16[64,4096]{1,0:T(8,128)(2,1)S(1)}, bf16[64,4096]{1,0:T(8,128)(2,1)}, u32[]{:S(2)}) copy-start(bf16[64,4096]{1,0:T(8,128)(2,1)} %param.17) | copy-start | bytes 1572868
  111.7 128.0 %reduce-scatter.5.cloned.1.call-start = ((), (), s32[]{:S(2)}) async-start(), calls=%async_computation.7 | async-start | bytes 2621440 | tf_op jit(solution)/shard_map/reduce_scatter | solution.py:100
  149.3 53.5 %copy-start.11 = (bf16[1,4096,512]{2,1,0:T(8,128)(2,1)S(1)}, bf16[1,4096,512]{2,1,0:T(8,128)(2,1)}, u32[]{:S(2)}) copy-start(bf16[1,4096,512]{2,1,0:T(8,128)(2,1)} %param.29) | copy-start | bytes 12582916
  202.9 2.2 copy-start.12
  205.1 2.2 copy-start.13
  207.2 38.1 %copy-start.9 = (f32[64,2]{0,1:T(2,128)S(1)}, f32[64,2]{0,1:T(2,128)}, u32[]{:S(2)}) copy-start(f32[64,2]{0,1:T(2,128)} %param.33) | copy-start | bytes 1540
  207.2 38.1 %slice-start = ((bf16[64,3,1024]{2,0,1:T(8,128)(2,1)}), bf16[64,2,1024]{2,0,1:T(8,128)(2,1)S(1)}, s32[]{:S(2)}) async-start(bf16[64,3,1024]{2,0,1:T(8,128)(2,1)} %param.19), calls=%async_computation.8 | async-start | bytes 524288 | tf_op jit(solution)/shard_map/slice | solution.py:63
  239.7 19.8 %all-to-all-start.2 = ((bf16[8,32,1024]{2,1,0:T(8,128)(2,1)}), bf16[8,32,1024]{2,1,0:T(8,128)(2,1)S(1)}, u32[]{:S(2)}, u32[]{:S(2)}) async-start(bf16[8,32,1024]{2,1,0:T(8,128)(2,1)} %reduce-scatter.5.cloned.1.call-done), calls=%async_computation.4 | async-start | bytes 1048576 | tf_op jit(solution)/shard_map/all_to_all | solution.py:103
Sparse Core Ops, SparseCore 0:
  36.5 67.3 reduce-scatter.2
  111.8 32.4 all-reduce.1
  210.0 29.6 reduce-scatter.4
where the time goes:
time: 269 us; the launch traced here: 268 us
  waiting for transfers between devices  142 us (53%)
  blocking collectives  74.4 us (28%)
  matrix products  16.6 us (6%)
  between operations  14.1 us (5%)
  other arithmetic  11.2 us (4%)
  starting transfers between devices  5.64 us (2%)
  local copies, waits for them, and re-layouts  3.75 us (1%)
    reduce_scatter x1, waiting for transfers between devices, shards(): lax.psum_scatter(jnp.dot(columns, joined, preferred_element_type=jnp.floa...  66.8 us
    all_to_all x1, blocking collectives, shards(): lax.all_to_all(send, 'ep', split_axis=0, concat_axis=0, tiled=True)  52.8 us
    psum x1, waiting for transfers between devices, shards(): lax.psum(partial_out.astype(jnp.bfloat16), 'tp').astype(jnp.float32)  32.4 us
    reduce_scatter x1, waiting for transfers between devices, shards(): lax.psum_scatter(partial_experts.astype(jnp.bfloat16), 'tp', scatter_dime...  29.8 us
    all_to_all x1, blocking collectives, shards(): lax.all_to_all(normed, 'ep', split_axis=1, concat_axis=0, tiled=True)  21.6 us
    all_to_all x1, waiting for transfers between devices, shards(): lax.all_to_all(reduced, 'ep', split_axis=0, concat_axis=0, tiled=True)  13.3 us
    dot_general x1, matrix products, shards(): partial_out = jnp.dot(gated, out_weight, preferred_element_type=jnp.float32)  5.88 us
    all_to_all x1, starting transfers between devices, shards(): lax.all_to_all(reduced, 'ep', split_axis=0, concat_axis=0, tiled=True)  5.51 us
  transfers between devices with their start and end apart: 4, of which 4 were waited for; matrix products, arithmetic and copies ran while one was open for 1% of the time, Pallas kernels for 0%

commit v1 on v0

--- a/solution.py
+++ b/solution.py
@@ -78,7 +78,9 @@
     ) * in_gate * conv.astype(jnp.float32)
     gated = (state_out * jax.nn.gelu(proj_y, approximate=True)).astype(jnp.bfloat16)
     partial_out = jnp.dot(gated, out_weight, preferred_element_type=jnp.float32)
-    mixed = base + lax.psum(partial_out.astype(jnp.bfloat16), "tp").astype(jnp.float32)
+    mixed = base + jax.lax.all_gather(partial_out.astype(jnp.bfloat16), "tp").sum(axis=0).astype(
+        jnp.float32
+    )
     normed2 = rms_scale(mixed, moe_gain).astype(jnp.bfloat16)
     experts = lax.axis_size("ep")
     topk = routes.shape[1]

time: 269 us -> 259 us (0.963)
  waiting for transfers between devices: 142 us -> 131 us
    psum x1 -> x0, waiting for transfers between devices: 32.4 us -> none  [shards(): lax.psum(partial_out.astype(jnp.bfloat16), 'tp').astype(jnp.float32)]
    all_gather x0 -> x1, waiting for transfers between devices: none -> 21 us  [shards(): jax.lax.all_gather(partial_out.astype(jnp.bfloat16), 'tp').sum(axis=0)]
where the time goes in v1:
time: 259 us; the launch traced here: 258 us
  waiting for transfers between devices  131 us (51%)
  blocking collectives  75.6 us (29%)
  matrix products  16.6 us (6%)
  between operations  14.1 us (5%)
  other arithmetic  11.1 us (4%)
  starting transfers between devices  5.63 us (2%)
  local copies, waits for them, and re-layouts  3.76 us (1%)
    reduce_scatter x1, waiting for transfers between devices, shards(): lax.psum_scatter(jnp.dot(columns, joined, preferred_element_type=jnp.floa...  67.6 us
    all_to_all x1, blocking collectives, shards(): lax.all_to_all(send, 'ep', split_axis=0, concat_axis=0, tiled=True)  54 us
    reduce_scatter x1, waiting for transfers between devices, shards(): lax.psum_scatter(partial_experts.astype(jnp.bfloat16), 'tp', scatter_dime...  29.4 us
    all_to_all x1, blocking collectives, shards(): lax.all_to_all(normed, 'ep', split_axis=1, concat_axis=0, tiled=True)  21.6 us
    all_gather x1, waiting for transfers between devices, shards(): jax.lax.all_gather(partial_out.astype(jnp.bfloat16), 'tp').sum(axis=0)  21 us
    all_to_all x1, waiting for transfers between devices, shards(): lax.all_to_all(reduced, 'ep', split_axis=0, concat_axis=0, tiled=True)  13.3 us
    dot_general x1, matrix products, shards(): partial_out = jnp.dot(gated, out_weight, preferred_element_type=jnp.float32)  5.89 us
    all_to_all x1, starting transfers between devices, shards(): lax.all_to_all(reduced, 'ep', split_axis=0, concat_axis=0, tiled=True)  5.51 us
  transfers between devices with their start and end apart: 4, of which 4 were waited for; matrix products, arithmetic and copies ran while one was open for 1% of the time, Pallas kernels for 0%

profile of v1, /device:TPU:0, one launch (start us, length us, event | category | flops | bytes accessed | tf_op | source)
XLA Modules:
  0.0 258.2 jit_solution(1924635877569639972)
XLA Ops:
  7.2 0.0 copy-start
  7.2 0.0 reduce-scatter.3.cloned.1.call-start
  7.2 0.7 convert_element_type.65
  8.0 1.2 fusion.23
  9.2 1.2 fusion.25
  10.5 21.6 %all_to_all.29 = bf16[64,8,512]{2,0,1:T(8,128)(2,1)S(1)} all-to-all(bf16[64,8,512]{2,0,1:T(8,128)(2,1)S(1)} %bitcast.87), channel_id=1, replica_groups=mesh['ep'=8,'tp'=4] {'ep'}, dimensions={1} | all-to-all | bytes 1048576 | tf_op jit(solution)/shard_map/all_to_all | solution.py:52
  32.1 4.2 %convolution_convert_fusion.3 = bf16[512,2048]{1,0:T(8,128)(2,1)} fusion(bf16[512,512]{1,0:T(8,128)(2,1)S(1)} %bitcast.90, bf16[512,1024]{1,0:T(8,128)(2,1)} %param.22, bf16[512,1024]{1,0:T(8,128)(2,1)} %param.21), kind=kOutput, calls=%fused_computation.8 | convolution fusion | flops 1078984704 | bytes 4718592 | tf_op jit(solution)/shard_map/dot_general | solution.py:55
  36.3 0.0 reduce-scatter.3.cloned.1.call-update
  36.3 0.0 all-gather.3.cloned.1.call-start
  36.4 0.1 convert_element_type.63
  36.5 67.6 %reduce-scatter.3.cloned.1.call-done = bf16[64,2048]{1,0:T(8,128)(2,1)} async-done(((bf16[512,2048]{1,0:T(8,128)(2,1)}), bf16[64,2048]{1,0:T(8,128)(2,1)}) %reduce-scatter.3.cloned.1.call-update) | async-done | bytes 262160 | tf_op jit(solution)/shard_map/reduce_scatter | solution.py:54
  104.1 1.1 fusion.36
  105.2 0.2 fusion.22
  105.5 0.2 fusion.18
  105.8 0.2 multiply_add_fusion
  106.0 0.0 copy-start.2
  106.0 0.0 copy-start.7
  106.0 0.0 copy-start.10
  106.0 0.0 copy-start.1
  106.1 5.9 %convolution_convert_fusion.2 = bf16[64,4096]{1,0:T(8,128)(2,1)} fusion(bf16[1024,4096]{1,0:T(8,128)(2,1)} %param.27, f32[64,1024]{1,0:T(8,128)S(1)} %multiply_add_fusion, bf16[64,2048]{1,0:T(8,128)(2,1)S(1)} %copy-done.4), kind=kOutput, calls=%fused_computation.2 | convolution fusion | flops 537853952 | bytes 9306112 | tf_op jit(solution)/shard_map/dot_general | solution.py:80
  112.0 0.0 all-gather.3.cloned.1.call-update
  112.0 0.0 reduce-scatter.5.cloned.1.call-start
  112.1 0.1 copy.43
  112.2 0.1 reshape.101
  112.3 0.1 fusion.52
  112.4 0.2 reduce_window_sum.11
  112.6 0.2 select_reduce_fusion
  112.8 21.0 %all-gather.3.cloned.1.call-done = bf16[256,4096]{1,0:T(8,128)(2,1)} async-done(((bf16[64,4096]{1,0:T(8,128)(2,1)}), bf16[256,4096]{1,0:T(8,128)(2,1)}) %all-gather.3.cloned.1.call-update) | async-done | bytes 2097168 | tf_op jit(solution)/shard_map/all_gather | solution.py:81
  133.8 2.0 reduce_sum.58
  135.8 1.3 convert_add_fusion
  137.1 0.2 multiply_convert_fusion
  137.3 1.0 broadcast_in_dim.4
  138.3 0.4 reshape.102
  138.8 0.7 convolution_convert_fusion
  139.5 54.0 %all_to_all.30 = bf16[8,32,4096]{2,1,0:T(8,128)(2,1)S(1)} all-to-all(bf16[8,32,4096]{2,1,0:T(8,128)(2,1)S(1)} %bitcast.81), channel_id=1, replica_groups=mesh['ep'=8,'tp'=4] {'ep'}, dimensions={0} | all-to-all | bytes 4194304 | tf_op jit(solution)/shard_map/all_to_all | solution.py:95
  193.5 1.2 fusion.3
  194.7 0.9 copy-done.12
  195.7 1.3 fusion.11
  196.9 0.9 copy-done.13
  197.9 2.6 %convolution_convert_fusion.1 = bf16[8,32,4096]{2,1,0:T(8,128)(2,1)} fusion(bf16[8,32,512]{2,1,0:T(8,128)(2,1)S(1)} %bitcast.97, bf16[1,512,4096]{2,1,0:T(8,128)(2,1)S(1)} %copy-done.13), kind=kOutput, calls=%fused_computation.1 | convolution fusion | flops 1074790400 | bytes 6553600 | tf_op jit(solution)/shard_map/dot_general | solution.py:100
  200.5 0.0 reduce-scatter.5.cloned.1.call-update
  200.5 29.4 %reduce-scatter.5.cloned.1.call-done = bf16[8,32,1024]{2,1,0:T(8,128)(2,1)} async-done(((bf16[8,32,4096]{2,1,0:T(8,128)(2,1)}), bf16[8,32,1024]{2,1,0:T(8,128)(2,1)}) %reduce-scatter.5.cloned.1.call-update) | async-done | bytes 524304 | tf_op jit(solution)/shard_map/reduce_scatter | solution.py:102
  229.9 5.5 %all-to-all-start.2 = ((bf16[8,32,1024]{2,1,0:T(8,128)(2,1)}), bf16[8,32,1024]{2,1,0:T(8,128)(2,1)S(1)}, u32[]{:S(2)}, u32[]{:S(2)}) async-start(bf16[8,32,1024]{2,1,0:T(8,128)(2,1)} %reduce-scatter.5.cloned.1.call-done), calls=%async_computation.4 | async-start | bytes 1048576 | tf_op jit(solution)/shard_map/all_to_all | solution.py:105
  235.4 0.1 iota_compare_fusion.1
  235.6 0.8 pad_maximum_fusion
  236.4 13.3 %all-to-all-done.2 = bf16[8,32,1024]{2,1,0:T(8,128)(2,1)S(1)} async-done(((bf16[8,32,1024]{2,1,0:T(8,128)(2,1)}), bf16[8,32,1024]{2,1,0:T(8,128)(2,1)S(1)}, u32[]{:S(2)}, u32[]{:S(2)}) %all-to-all-start.2) | async-done | bytes 524320 | tf_op jit(solution)/shard_map/all_to_all | solution.py:105
  249.7 0.2 fusion.14
  250.0 1.6 add_convert_fusion
  (38 shorter events, 0.3 us)
Async XLA Ops:
  7.2 98.0 %copy-start = (bf16[4,256,256]{2,1,0:T(8,128)(2,1)S(1)}, bf16[4,256,256]{2,1,0:T(8,128)(2,1)}, u32[]{:S(2)}) copy-start(bf16[4,256,256]{2,1,0:T(8,128)(2,1)} %param.24) | copy-start | bytes 1572868
  7.2 96.9 %reduce-scatter.3.cloned.1.call-start = ((), (), s32[]{:S(2)}) async-start(), calls=%async_computation.5 | async-start | bytes 2359296 | tf_op jit(solution)/shard_map/reduce_scatter | solution.py:54
  32.1 4.3 %copy-start.3 = (bf16[64,3,1024]{2,0,1:T(8,128)(2,1)S(1)}, bf16[64,3,1024]{2,0,1:T(8,128)(2,1)}, u32[]{:S(2)}) copy-start(bf16[64,3,1024]{2,0,1:T(8,128)(2,1)} %param.19) | copy-start | bytes 1179652
  32.1 4.4 %copy-start.8 = (f32[1024]{0:T(1024)S(1)}, f32[1024]{0:T(1024)}, u32[]{:S(2)}) copy-start(f32[1024]{0:T(1024)} %param.26) | copy-start | bytes 12292
  32.1 4.4 %copy-start.6 = (bf16[4,1024]{1,0:T(4,128)(2,1)S(1)}, bf16[4,1024]{1,0:T(4,128)(2,1)}, u32[]{:S(2)}) copy-start(bf16[4,1024]{1,0:T(4,128)(2,1)} %param.23) | copy-start | bytes 24580
  36.3 69.2 %copy-start.14 = (bf16[4,256,256]{2,1,0:T(8,128)(2,1)S(1)}, bf16[4,256,256]{2,1,0:T(8,128)(2,1)}, u32[]{:S(2)}) copy-start(bf16[4,256,256]{2,1,0:T(8,128)(2,1)} %param.25) | copy-start | bytes 1572868
  36.3 69.4 %copy-start.5 = (f32[64,1024]{1,0:T(8,128)S(1)}, f32[64,1024]{1,0:T(8,128)}, u32[]{:S(2)}) copy-start(f32[64,1024]{1,0:T(8,128)} %param.18) | copy-start | bytes 786436
  36.3 97.4 %all-gather.3.cloned.1.call-start = ((), (), s32[]{:S(2)}) async-start(), calls=%async_computation.7 | async-start | bytes 2621440 | tf_op jit(solution)/shard_map/all_gather | solution.py:81
  104.1 1.9 copy-start.4
  106.0 5.9 %copy-start.2 = (f32[64,1024]{1,0:T(8,128)}, f32[64,1024]{1,0:T(8,128)S(1)}, u32[]{:S(2)}) copy-start(f32[64,1024]{1,0:T(8,128)S(1)} %multiply_add_fusion) | copy-start | bytes 786436
  106.0 6.0 %copy-start.7 = (bf16[4096]{0:T(1024)(128)(2,1)S(1)}, bf16[4096]{0:T(1024)(128)(2,1)}, u32[]{:S(2)}) copy-start(bf16[4096]{0:T(1024)(128)(2,1)} %param.28) | copy-start | bytes 24580
  106.0 6.0 %copy-start.10 = (s32[64,2]{0,1:T(2,128)S(1)}, s32[64,2]{0,1:T(2,128)}, u32[]{:S(2)}) copy-start(s32[64,2]{0,1:T(2,128)} %param.32) | copy-start | bytes 1540
  106.0 29.7 %copy-start.1 = (bf16[64,4096]{1,0:T(8,128)(2,1)S(1)}, bf16[64,4096]{1,0:T(8,128)(2,1)}, u32[]{:S(2)}) copy-start(bf16[64,4096]{1,0:T(8,128)(2,1)} %param.17) | copy-start | bytes 1572868
  112.0 117.9 %reduce-scatter.5.cloned.1.call-start = ((), (), s32[]{:S(2)}) async-start(), calls=%async_computation.6 | async-start | bytes 2621440 | tf_op jit(solution)/shard_map/reduce_scatter | solution.py:102
  138.7 54.7 %copy-start.11 = (bf16[1,4096,512]{2,1,0:T(8,128)(2,1)S(1)}, bf16[1,4096,512]{2,1,0:T(8,128)(2,1)}, u32[]{:S(2)}) copy-start(bf16[1,4096,512]{2,1,0:T(8,128)(2,1)} %param.29) | copy-start | bytes 12582916
  193.5 2.2 copy-start.12
  195.7 2.2 copy-start.13
  197.9 37.7 %copy-start.9 = (f32[64,2]{0,1:T(2,128)S(1)}, f32[64,2]{0,1:T(2,128)}, u32[]{:S(2)}) copy-start(f32[64,2]{0,1:T(2,128)} %param.33) | copy-start | bytes 1540
  197.9 37.8 %slice-start = ((bf16[64,3,1024]{2,0,1:T(8,128)(2,1)}), bf16[64,2,1024]{2,0,1:T(8,128)(2,1)S(1)}, s32[]{:S(2)}) async-start(bf16[64,3,1024]{2,0,1:T(8,128)(2,1)} %param.19), calls=%async_computation.8 | async-start | bytes 524288 | tf_op jit(solution)/shard_map/slice | solution.py:63
  229.9 19.8 %all-to-all-start.2 = ((bf16[8,32,1024]{2,1,0:T(8,128)(2,1)}), bf16[8,32,1024]{2,1,0:T(8,128)(2,1)S(1)}, u32[]{:S(2)}, u32[]{:S(2)}) async-start(bf16[8,32,1024]{2,1,0:T(8,128)(2,1)} %reduce-scatter.5.cloned.1.call-done), calls=%async_computation.4 | async-start | bytes 1048576 | tf_op jit(solution)/shard_map/all_to_all | solution.py:105
Sparse Core Ops, SparseCore 0:
  36.5 67.5 reduce-scatter.2
  112.1 21.6 all-gather.2
  200.6 29.2 reduce-scatter.4
